TPU v7x, 256 devices: a whole 4x4x8 slice. The times are simulated.
256 devices in a mesh: ep: 128 (over z, y, x), tp: 2 (over core).
Axes of the slice: x: 4, y: 4, z: 8, core: 2. Of those that a mesh axis runs over, the one named last changes fastest.
Arguments:
- tokens: bfloat16 [4096, 1024], P('ep'), may hold values from -6 to 6
- norm_gain: float32 [1024], replicated, may hold values from 0.1 to 1.9
- routing: int32 [4096, 4], P('ep'), may hold values from 0 to 127, all different within a row; in each aligned block of 32 rows (0 to 31, 32 to 63, ...) at most 16 rows name the same one
- route_logits: float32 [4096, 4], P('ep'), may hold values from -6 to 6
- w_gate: bfloat16 [128, 1024, 1024], P('ep', None, 'tp'), may hold values from -0.1875 to 0.1875
- w_up: bfloat16 [128, 1024, 1024], P('ep', None, 'tp'), may hold values from -0.1875 to 0.1875
- w_down: bfloat16 [128, 1024, 1024], P('ep', None, 'tp'), may hold values from -0.1875 to 0.1875
Outputs:
- mixed: bfloat16 [4096, 1024], P('ep', 'tp')
Inputs may be any that keep to these rules, and one draw needn't show every extreme that they name: `routing`: each row names 4 different experts; among the 32 tokens of one index of ep (aligned blocks of rows) no expert is named by more than 16 rows, and some block has an expert named by exactly 16.
All inputs are finite; a program needn't handle non-finite values.
Results may differ from a plain program's by a relative error of at most 0.0085.
Values may be sent and summed in bfloat16 or wider, within the bound.
No kernel may reach another device: no remote copies, remote signals or barrier semaphores. Data moves between devices by JAX's collectives and lax.ppermute only.
A program may use at most 64 MiB of HBM per device.

v0:
```python
import jax
import jax.numpy as jnp
from jax import lax
from jax.sharding import PartitionSpec as P

CAP = 16


eps = 1e-05


def taken_in(share, axis, dim, step, start):
    def gathered(part):
        return lax.all_gather(part, axis, axis=dim, tiled=True)

    return step(start, jax.tree.map(gathered, share), jnp.int32(0))


def clamped(gate_part, up_part):
    limited = jnp.minimum(gate_part, 7.0)
    linear = jnp.clip(up_part, -7.0, 7.0)
    return limited * jax.nn.sigmoid(1.702 * limited) * (linear + 1.0)


def expert_rows(rows, w_gate, w_up, w_down):
    gate_part = jnp.dot(rows, w_gate[0], preferred_element_type=jnp.float32)
    up_part = jnp.dot(rows, w_up[0], preferred_element_type=jnp.float32)
    hidden = clamped(gate_part, up_part).astype(jnp.bfloat16)
    down_local = w_down[0]
    empty = jnp.zeros((rows.shape[0], down_local.shape[1]), jnp.float32)

    def add_rows(total, piece, start):
        weights = lax.dynamic_slice_in_dim(down_local, start, piece.shape[1], 0)
        return total + jnp.dot(piece, weights, preferred_element_type=jnp.float32)

    summed = taken_in(hidden, "tp", 1, add_rows, empty)
    return summed.astype(jnp.bfloat16)


def shards(tokens, norm_gain, routing, route_logits, w_gate, w_up, w_down):
    as_float = tokens.astype(jnp.float32)
    scaled = as_float * lax.rsqrt(jnp.mean(as_float * as_float, axis=-1, keepdims=True) + eps)
    normed = (scaled * norm_gain).astype(jnp.bfloat16)
    gate_probs = jax.nn.softmax(route_logits, axis=-1)
    tok_dev = tokens.shape[0]
    topk = routing.shape[1]
    width = tokens.shape[1]
    n_ep = lax.axis_size("ep")
    assigns = tok_dev * topk
    flat_e = routing.reshape(-1)
    onehot = (flat_e[:, None] == jnp.arange(n_ep, dtype=jnp.int32)[None, :]).astype(jnp.int32)
    slot_rank = jnp.sum((jnp.cumsum(onehot, axis=0) - onehot) * onehot, axis=1).astype(jnp.int32)
    slot_index = flat_e * CAP + slot_rank
    flat_tok = jnp.arange(assigns, dtype=jnp.int32) // topk
    outbound = jnp.zeros((n_ep * CAP, width), jnp.bfloat16).at[slot_index].set(normed[flat_tok])
    arrived = lax.all_to_all(
        outbound.reshape(n_ep, CAP, width), "ep", split_axis=0, concat_axis=0, tiled=True
    )
    expert_out = expert_rows(arrived.reshape(n_ep * CAP, width), w_gate, w_up, w_down)
    half_width = expert_out.shape[1]
    returned_rows = lax.all_to_all(
        expert_out.reshape(n_ep, CAP, half_width), "ep", split_axis=0, concat_axis=0, tiled=True
    )
    returned_rows = returned_rows.reshape(n_ep * CAP, half_width)
    picked = returned_rows[slot_index].astype(jnp.float32) * gate_probs.reshape(-1)[:, None]
    mixed = jnp.sum(picked.reshape(tok_dev, topk, half_width), axis=1).astype(jnp.bfloat16)
    return mixed


def solution(mesh):
    return jax.shard_map(
        shards,
        mesh=mesh,
        in_specs=(
            P("ep", None),
            P(),
            P("ep", None),
            P("ep", None),
            P("ep", None, "tp"),
            P("ep", None, "tp"),
            P("ep", None, "tp"),
        ),
        out_specs=P("ep", "tp"),
        check_vma=False,
    )
```

profile of v0, /device:TPU:1, one launch (start us, length us, event | category | flops | bytes accessed | tf_op | source)
XLA Modules:
  0.0 233.8 jit_solution(14845142519807675940)
XLA Ops:
  6.5 0.0 copy-start
  6.5 0.0 all-gather.2.cloned.1.call-start
  6.5 0.8 copy.12
  7.4 0.7 broadcast_multiply_fusion
  8.1 0.1 eq.15
  8.2 0.1 fusion.10
  8.3 0.2 reduce_window_sum.11
  8.5 0.2 select_reduce_fusion
  8.6 0.1 copy.11
  8.7 0.1 mul.61
  8.8 1.0 fusion.7
  9.8 0.9 fusion.9
  10.8 4.8 %scatter_custom_fusion = bf16[2048,1024]{1,0:T(8,128)(2,1)} fusion(s32[128]{0:T(128)S(1)} %fusion.14, bf16[]{:T(256)} %constant.17.clone.1, bf16[32,1024]{1,0:T(8,128)(2,1)S(1)} %fusion.9, s32[1024]{0:T(1024)S(1)} %pad_clamp_fusion.1), kind=kCustom, calls=%fused_computation.5 | custom fusion | bytes 4194306 | tf_op jit(solution)/shard_map/scatter | solution.py:55
  15.5 111.8 %all_to_all.10 = bf16[128,16,1024]{2,1,0:T(8,128)(2,1)S(1)} all-to-all(bf16[128,16,1024]{2,1,0:T(8,128)(2,1)} %bitcast.24), channel_id=1, replica_groups=mesh['ep'=128,'tp'=2] {'ep'}, dimensions={0} | all-to-all | bytes 8388608 | tf_op jit(solution)/shard_map/all_to_all | solution.py:56
  127.3 0.0 copy-done
  127.3 0.0 copy-start.2
  127.3 2.3 %fusion.4 = f32[2048,512]{1,0:T(8,128)S(1)} fusion(bf16[2048,1024]{1,0:T(8,128)(2,1)S(1)} %bitcast.26, bf16[1,1024,512]{2,1,0:T(8,128)(2,1)S(1)} %copy-done), kind=kOutput, calls=%fused_computation.9 | convolution fusion | flops 2147483648 | bytes 9437184 | tf_op jit(solution)/shard_map/dot_general | solution.py:26
  129.7 0.0 copy-done.2
  129.7 0.0 copy-start.3
  129.7 4.8 %multiply_convert_fusion = bf16[2048,512]{1,0:T(8,128)(2,1)} fusion(f32[2048,512]{1,0:T(8,128)S(1)} %fusion.4, bf16[2048,1024]{1,0:T(8,128)(2,1)S(1)} %bitcast.27, bf16[1,1024,512]{2,1,0:T(8,128)(2,1)S(1)} %copy-done.2), kind=kOutput, calls=%fused_computation.3 | convolution fusion | flops 2157969408 | bytes 11534336 | tf_op jit(solution)/shard_map/dot_general | solution.py:27
  134.6 0.0 all-gather.2.cloned.1.call-update
  134.6 18.6 %all-gather.2.cloned.1.call-done = bf16[2048,1024]{1,0:T(8,128)(2,1)} async-done(((bf16[2048,512]{1,0:T(8,128)(2,1)}), bf16[2048,1024]{1,0:T(8,128)(2,1)}) %all-gather.2.cloned.1.call-update) | async-done | bytes 4194320 | tf_op jit(solution)/shard_map/all_gather | solution.py:14
  153.2 0.0 copy-done.3
  153.2 5.9 %convolution_convert_fusion = bf16[2048,512]{1,0:T(8,128)(2,1)} fusion(bf16[2048,1024]{1,0:T(8,128)(2,1)} %all-gather.2.cloned.1.call-done, bf16[1,1024,512]{2,1,0:T(8,128)(2,1)S(1)} %copy-done.3), kind=kOutput, calls=%fused_computation.4 | convolution fusion | flops 2148532224 | bytes 7340032 | tf_op jit(solution)/shard_map/dot_general | solution.py:34
  159.1 0.0 copy-start.1
  159.1 13.7 %all-to-all-start.1 = ((bf16[128,16,512]{2,1,0:T(8,128)(2,1)}), bf16[128,16,512]{2,1,0:T(8,128)(2,1)S(1)}, u32[]{:S(2)}, u32[]{:S(2)}) async-start(bf16[128,16,512]{2,1,0:T(8,128)(2,1)} %bitcast.28), calls=%async_computation.1 | async-start | bytes 4194304 | tf_op jit(solution)/shard_map/all_to_all | solution.py:61
  172.7 0.0 copy-done.1
  172.8 0.1 copy.13
  172.9 52.2 %all-to-all-done.1 = bf16[128,16,512]{2,1,0:T(8,128)(2,1)S(1)} async-done(((bf16[128,16,512]{2,1,0:T(8,128)(2,1)}), bf16[128,16,512]{2,1,0:T(8,128)(2,1)S(1)}, u32[]{:S(2)}, u32[]{:S(2)}) %all-to-all-start.1) | async-done | bytes 2097184 | tf_op jit(solution)/shard_map/all_to_all | solution.py:61
  225.1 0.8 gather_fusion
  226.0 0.1 reshape.110
  226.1 0.8 multiply_reduce_fusion
  (8 shorter events, 0.1 us)
Async XLA Ops:
  6.5 120.8 %copy-start = (bf16[1,1024,512]{2,1,0:T(8,128)(2,1)S(1)}, bf16[1,1024,512]{2,1,0:T(8,128)(2,1)}, u32[]{:S(2)}) copy-start(bf16[1,1024,512]{2,1,0:T(8,128)(2,1)} %param.11) | copy-start | bytes 3145732
  6.5 146.6 %all-gather.2.cloned.1.call-start = ((), (), s32[]{:S(2)}) async-start(), calls=%async_computation.2 | async-start | bytes 6291456 | tf_op jit(solution)/shard_map/all_gather | solution.py:14
  127.3 2.3 %copy-start.2 = (bf16[1,1024,512]{2,1,0:T(8,128)(2,1)S(1)}, bf16[1,1024,512]{2,1,0:T(8,128)(2,1)}, u32[]{:S(2)}) copy-start(bf16[1,1024,512]{2,1,0:T(8,128)(2,1)} %param.12) | copy-start | bytes 3145732
  129.7 23.5 %copy-start.3 = (bf16[1,1024,512]{2,1,0:T(8,128)(2,1)S(1)}, bf16[1,1024,512]{2,1,0:T(8,128)(2,1)}, u32[]{:S(2)}) copy-start(bf16[1,1024,512]{2,1,0:T(8,128)(2,1)} %param.13) | copy-start | bytes 3145732
  159.1 13.7 %copy-start.1 = (f32[32,4]{0,1:T(4,128)S(1)}, f32[32,4]{0,1:T(4,128)}, u32[]{:S(2)}) copy-start(f32[32,4]{0,1:T(4,128)} %param.10) | copy-start | bytes 1540
  159.1 66.1 %all-to-all-start.1 = ((bf16[128,16,512]{2,1,0:T(8,128)(2,1)}), bf16[128,16,512]{2,1,0:T(8,128)(2,1)S(1)}, u32[]{:S(2)}, u32[]{:S(2)}) async-start(bf16[128,16,512]{2,1,0:T(8,128)(2,1)} %bitcast.28), calls=%async_computation.1 | async-start | bytes 4194304 | tf_op jit(solution)/shard_map/all_to_all | solution.py:61
Sparse Core Ops, SparseCore 0:
  134.7 18.4 all-gather.1
where the time goes:
time: 234 us
  blocking collectives  112 us (48%)
  waiting for transfers between devices  70.8 us (30%)
  starting transfers between devices  13.7 us (6%)
  between operations  13.5 us (6%)
  matrix products  13.1 us (6%)
  local copies, waits for them, and re-layouts  6.95 us (3%)
  other arithmetic  3.94 us (2%)
    all_to_all x1, blocking collectives, shards(): lax.all_to_all(outbound.reshape(n_ep, CAP, width), 'ep', split_axis=0, co...  112 us
    all_to_all x1, waiting for transfers between devices, shards(): lax.all_to_all(expert_out.reshape(n_ep, CAP, half_width), 'ep', split_axi...  52.2 us
    all_gather x1, waiting for transfers between devices, gathered(): return lax.all_gather(part, axis, axis=dim, tiled=True)  18.6 us
    all_to_all x1, starting transfers between devices, shards(): lax.all_to_all(expert_out.reshape(n_ep, CAP, half_width), 'ep', split_axi...  13.7 us
    dot_general x1, matrix products, add_rows(): return total + jnp.dot(piece, weights, preferred_element_type=jnp.float32)  5.87 us
    dot_general x1, matrix products, expert_rows(): up_part = jnp.dot(rows, w_up[0], preferred_element_type=jnp.float32)  4.84 us
    scatter x1, local copies, waits for them, and re-layouts, shards(): jnp.zeros((n_ep * CAP, width), jnp.bfloat16).at[slot_index]  4.75 us
  transfers between devices with their start and end apart: 2, of which 2 were waited for; matrix products, arithmetic and copies ran while one was open for 0% of the time, Pallas kernels for 0%

commit v1 on v0

v1 whole, which is shorter than its diff:
```python
import jax
import jax.numpy as jnp
from jax import lax
from jax.sharding import PartitionSpec as P

eps = 1e-05


def clamped(gate_part, up_part):
    limited = jnp.minimum(gate_part, 7.0)
    linear = jnp.clip(up_part, -7.0, 7.0)
    return limited * jax.nn.sigmoid(1.702 * limited) * (linear + 1.0)


def shards(tokens, norm_gain, routing, route_logits, w_gate, w_up, w_down):
    core = lax.axis_index("tp")
    expert = lax.axis_index("ep")
    half = tokens.shape[0] // 2
    width = tokens.shape[1]
    mine = lax.dynamic_slice_in_dim(tokens, core * half, half, 0)
    routes = lax.dynamic_slice_in_dim(routing, core * half, half, 0)
    logits = lax.dynamic_slice_in_dim(route_logits, core * half, half, 0)

    gate_full = lax.all_gather(w_gate[0], "tp", axis=1, tiled=True)
    up_full = lax.all_gather(w_up[0], "tp", axis=1, tiled=True)
    down_full = lax.all_gather(w_down[0], "tp", axis=1, tiled=True)

    as_float = mine.astype(jnp.float32)
    scaled = as_float * lax.rsqrt(jnp.mean(as_float * as_float, axis=-1, keepdims=True) + eps)
    normed = (scaled * norm_gain).astype(jnp.bfloat16)
    probs = jax.nn.softmax(logits, axis=-1)

    rows = lax.all_gather(normed, "ep", axis=0, tiled=True)
    all_routes = lax.all_gather(routes, "ep", axis=0, tiled=True)
    all_probs = lax.all_gather(probs, "ep", axis=0, tiled=True)
    share = jnp.sum(jnp.where(all_routes == expert, all_probs, 0.0), axis=1, keepdims=True)

    gate_part = jnp.dot(rows, gate_full, preferred_element_type=jnp.float32)
    up_part = jnp.dot(rows, up_full, preferred_element_type=jnp.float32)
    hidden = clamped(gate_part, up_part).astype(jnp.bfloat16)
    out = jnp.dot(hidden, down_full, preferred_element_type=jnp.float32)
    out = (out * share).astype(jnp.bfloat16)
    mixed = lax.psum_scatter(out, "ep", scatter_dimension=0, tiled=True)
    return lax.all_to_all(mixed, "tp", split_axis=1, concat_axis=0, tiled=True)


def solution(mesh):
    return jax.shard_map(
        shards,
        mesh=mesh,
        in_specs=(
            P("ep", None),
            P(),
            P("ep", None),
            P("ep", None),
            P("ep", None, "tp"),
            P("ep", None, "tp"),
            P("ep", None, "tp"),
        ),
        out_specs=P("ep", "tp"),
        check_vma=False,
    )
```

time: 234 us -> 1440 us (6.15)
  waiting for transfers between devices: 70.8 us -> 709 us
  blocking collectives: 112 us -> 690 us
    reduce_scatter x0 -> x1, waiting for transfers between devices: none -> 707 us  [shards(): mixed = lax.psum_scatter(out, 'ep', scatter_dimension=0, tiled=True)]
    all_gather x0 -> x2, blocking collectives: none -> 580 us  [the longest x1 295 us: shards(): all_routes = lax.all_gather(routes, 'ep', axis=0, tiled=True)]
    all_to_all x1 -> x0, waiting for transfers between devices: 52.2 us -> none  [shards(): lax.all_to_all(expert_out.reshape(n_ep, CAP, half_width), 'ep', split_axi...]
    all_gather x1 -> x4, waiting for transfers between devices: 18.6 us -> 0.03 us  [the longest x1 0.02 us: shards(): rows = lax.all_gather(normed, 'ep', axis=0, tiled=True)]
  transfers between devices with their start and end apart: 2 -> 5, of which waited for: 2 -> 1; matrix products, arithmetic and copies ran while one was open for 0% -> 1% of each run, Pallas kernels for 0% -> 0%
where the time goes in v1:
time: 1440 us
  waiting for transfers between devices  709 us (49%)
  blocking collectives  690 us (48%)
  matrix products  25.4 us (2%)
    reduce_scatter x1, waiting for transfers between devices, shards(): mixed = lax.psum_scatter(out, 'ep', scatter_dimension=0, tiled=True)  707 us
    all_gather x1, blocking collectives, shards(): all_routes = lax.all_gather(routes, 'ep', axis=0, tiled=True)  295 us
    all_gather x1, blocking collectives, shards(): all_probs = lax.all_gather(probs, 'ep', axis=0, tiled=True)  284 us
    all_to_all x1, blocking collectives, shards(): return lax.all_to_all(mixed, 'tp', split_axis=1, concat_axis=0, tiled=True)  110 us
  transfers between devices with their start and end apart: 5, of which 1 were waited for; matrix products, arithmetic and copies ran while one was open for 1% of the time, Pallas kernels for 0%

profile of v1, /device:TPU:1, one launch (start us, length us, event | category | flops | bytes accessed | tf_op | source)
XLA Modules:
  0.0 1444.3 jit_solution(11463665645735502093)
XLA Ops:
  6.5 0.0 copy-start
  6.5 0.0 all-gather.12.cloned.1.call-start
  6.5 0.7 all-gather.12.cloned.1.call-update
  7.3 0.0 all-gather.10.cloned.1.call-start
  7.3 0.9 fusion.5
  8.2 1.5 fusion.7
  9.7 0.0 all-gather.10.cloned.1.call-update
  9.7 0.0 all-gather.14.cloned.1.call-start
  9.7 0.7 all-gather.14.cloned.1.call-update
  10.4 0.0 all-gather.16.cloned.1.call-start
  10.5 0.5 all-gather.16.cloned.1.call-update
  11.0 0.0 reduce-scatter.2.cloned.1.call-start
  11.1 0.8 dynamic-slice_reduce_fusion
  11.8 0.0 copy-done
  11.8 0.1 dynamic-slice_bitcast_fusion
  11.9 295.5 %all-gather.3 = s32[128,16,4]{1,2,0:T(4,128)S(1)} all-gather(s32[1,16,4]{1,2,0:T(4,128)S(1)} %dynamic-slice_bitcast_fusion), channel_id=1, replica_groups=mesh['ep'=128,'tp'=2] {'ep'}, dimensions={0}, use_global_device_ids=true | all-gather | bytes 33024 | tf_op jit(solution)/shard_map/all_gather | solution.py:34
  307.4 0.8 fusion.8
  308.1 0.8 divide_bitcast_fusion
  308.9 284.3 %all-gather.4 = f32[128,16,4]{1,2,0:T(4,128)S(1)} all-gather(f32[1,16,4]{1,2,0:T(4,128)S(1)} %divide_bitcast_fusion), channel_id=1, replica_groups=mesh['ep'=128,'tp'=2] {'ep'}, dimensions={0}, use_global_device_ids=true | all-gather | bytes 33024 | tf_op jit(solution)/shard_map/all_gather | solution.py:35
  593.2 0.2 select_reduce_fusion
  593.4 0.1 reshape.26
  593.5 0.0 all-gather.12.cloned.1.call-done
  593.5 0.0 all-gather.10.cloned.1.call-done
  593.6 10.6 fusion.3
  604.2 0.0 all-gather.14.cloned.1.call-done
  604.2 0.0 all-gather.16.cloned.1.call-done
  604.2 14.8 %multiply_convert_fusion = bf16[2048,1024]{1,0:T(8,128)(2,1)} fusion(f32[2048]{0:T(1024)S(1)} %reshape.26, f32[2048,1024]{1,0:T(8,128)} %fusion.3, bf16[2048,1024]{1,0:T(8,128)(2,1)} %all-gather.10.cloned.1.call-done, bf16[1,1024,1024]{2,1,0:T(8,128)(2,1)} %all-gather.16.cloned.1.call-done, bf16[1,1024,1024]{2,1,0:T(8,128)(2,1)} %all-gather.14.cloned.1.call-done), kind=kOutput, calls=%fused_computation | convolution fusion | flops 8615100416 | bytes 20979712 | tf_op jit(solution)/shard_map/dot_general | solution.py:41
  618.9 0.0 reduce-scatter.2.cloned.1.call-update
  619.0 707.2 %reduce-scatter.2.cloned.1.call-done = bf16[16,1024]{1,0:T(8,128)(2,1)} async-done(((bf16[2048,1024]{1,0:T(8,128)(2,1)}), bf16[16,1024]{1,0:T(8,128)(2,1)}) %reduce-scatter.2.cloned.1.call-update) | async-done | bytes 32784 | tf_op jit(solution)/shard_map/reduce_scatter | solution.py:43
  1326.1 0.8 copy.13
  1326.9 110.3 %all_to_all.19 = bf16[16,2,512]{2,0,1:T(8,128)(2,1)S(1)} all-to-all(bf16[16,2,512]{2,0,1:T(8,128)(2,1)S(1)} %bitcast.23), channel_id=1, replica_groups=mesh['ep'=128,'tp'=2] {'tp'}, dimensions={1} | all-to-all | bytes 65536 | tf_op jit(solution)/shard_map/all_to_all | solution.py:44
  1437.2 0.6 copy.15
  (1 shorter events, 0.0 us)
Async XLA Ops:
  6.5 5.3 copy-start
  6.5 587.0 %all-gather.12.cloned.1.call-start = ((), (), s32[]{:S(2)}) async-start(), calls=%async_computation.4 | async-start | bytes 3145728 | tf_op jit(solution)/shard_map/all_gather | solution.py:24
  7.3 586.3 %all-gather.10.cloned.1.call-start = ((), (), s32[]{:S(2)}) async-start(), calls=%async_computation.2 | async-start | bytes 4227072 | tf_op jit(solution)/shard_map/all_gather | solution.py:33
  9.7 594.5 %all-gather.14.cloned.1.call-start = ((), (), s32[]{:S(2)}) async-start(), calls=%async_computation.5 | async-start | bytes 3145728 | tf_op jit(solution)/shard_map/all_gather | solution.py:25
  10.4 593.7 %all-gather.16.cloned.1.call-start = ((), (), s32[]{:S(2)}) async-start(), calls=%async_computation.6 | async-start | bytes 3145728 | tf_op jit(solution)/shard_map/all_gather | solution.py:26
  11.0 1315.1 %reduce-scatter.2.cloned.1.call-start = ((), (), s32[]{:S(2)}) async-start(), calls=%async_computation.3 | async-start | bytes 4227072 | tf_op jit(solution)/shard_map/reduce_scatter | solution.py:43
Sparse Core Ops, SparseCore 0:
  9.1 20.4 all-gather.11
  33.2 113.1 all-gather.9
  148.2 17.7 all-gather.13
  167.6 17.1 all-gather.15
  619.1 706.9 reduce-scatter.1
